TPU v7x, 512 devices: a whole 4x4x16 slice. The times are simulated.
512 devices in a mesh: kv: 16 (over y, x), tp: 32 (over z, core).
Axes of the slice: x: 4, y: 4, z: 16, core: 2. Of those that a mesh axis runs over, the one named last changes fastest.
Arguments:
- residual: bfloat16 [512, 2048], P('tp', 'kv'), may hold values from -64 to 64
- prior_state: float32 [512, 16, 128, 128], P('tp', 'kv'), may hold values from -6 to 6
- w_query: bfloat16 [2048, 2048], P('tp', 'kv'), may hold values from -0.125 to 0.125
- w_forget: bfloat16 [2048, 2048], P('tp', 'kv'), may hold values from -0.125 to 0.125
- w_value: bfloat16 [2048, 2048], P('tp', 'kv'), may hold values from -0.125 to 0.125
- w_outgate: bfloat16 [2048, 2048], P('tp', 'kv'), may hold values from -0.125 to 0.125
- forget_floor: float32 [2048], P('kv'), may hold values from 0.05 to 0.9
- group_gain: float32 [2048], P('kv'), may hold values from 0.1 to 1.9
- w_mix_out: bfloat16 [2048, 2048], P('kv', 'tp'), may hold values from -0.397747564 to 0.397747564
- gain_mix_pre: float32 [2048], replicated, may hold values from 0.1 to 1.9
- gain_mix_post: float32 [2048], replicated, may hold values from 0.05 to 1.9
- gain_mlp_pre: float32 [2048], replicated, may hold values from 0.1 to 1.9
- gain_mlp_post: float32 [2048], replicated, may hold values from 0.1 to 1.9
- w_up: bfloat16 [2048, 8192], P('tp', 'kv'), may hold values from -0.125 to 0.125
- w_down: bfloat16 [8192, 2048], P('kv', 'tp'), may hold values from -0.198873782 to 0.198873782
Outputs:
- layer_out: bfloat16 [512, 2048], P('tp', 'kv')
- new_state: float32 [512, 16, 128, 128], P('tp', 'kv')
All inputs are finite; a program needn't handle non-finite values.
Results may differ from a plain program's by a relative error of at most 0.015.
Values may be sent and summed in bfloat16 or wider, within the bound.
No kernel may reach another device: no remote copies, remote signals or barrier semaphores. Data moves between devices by JAX's collectives and lax.ppermute only.
A program may use at most 64 MiB of HBM per device.

v0:
```python
import jax
import jax.numpy as jnp
from jax import lax
from jax.sharding import PartitionSpec as P

HEAD_DIM = 128


epsilon = 1e-06


def side_by_side(arrays, axis, dim, along):
    widths = [a.shape[along] for a in arrays]
    both = jnp.concatenate(arrays, axis=along)
    filled = lax.all_gather(both, axis, axis=dim, tiled=True)
    return tuple(jnp.split(filled, [sum(widths[:k]) for k in range(1, len(widths))], axis=along))


def split_up(value, dim, devices):
    before, after = (value.shape[:dim], value.shape[dim + 1 :])
    return jnp.moveaxis(value.reshape(*before, devices, -1, *after), dim, 0)


def summed_on_arrival(value, axis, dim):
    devices = lax.axis_size(axis)
    blocks = lax.all_to_all(split_up(value, dim, devices), axis, 0, 0, tiled=True)
    return jnp.sum(blocks, axis=0)


def from_everyone(value, axis):
    devices = lax.axis_size(axis)
    return lax.all_to_all(
        jnp.broadcast_to(value[None], (devices, *value.shape)), axis, 0, 0, tiled=True
    )


def taken_together(value, axis):
    return from_everyone(value, axis).sum(axis=0)


def inverse_norm(values):
    return lax.rsqrt(jnp.mean(values * values, axis=-1, keepdims=True) + epsilon)


def shards(
    residual,
    prior_state,
    w_query,
    w_forget,
    w_value,
    w_outgate,
    forget_floor,
    group_gain,
    w_mix_out,
    gain_mix_pre,
    gain_mix_post,
    gain_mlp_pre,
    gain_mlp_post,
    w_up,
    w_down,
):
    batch_rows = residual.shape[0]
    own_cols = residual.shape[1]
    offset = lax.axis_index("kv") * own_cols
    whole_rows = lax.all_gather(residual, "kv", axis=1, tiled=True)
    full_width = whole_rows.shape[1]
    stream = whole_rows.astype(jnp.float32)
    normed = (stream * inverse_norm(stream) * gain_mix_pre).astype(jnp.bfloat16)
    pieces = side_by_side((w_query, w_forget, w_value, w_outgate), "tp", 0, 1)
    left_part = normed
    totals = tuple(
        (
            jnp.dot(left_part, weight_part, preferred_element_type=jnp.float32)
            for weight_part in pieces
        )
    )
    query_pre, forget_pre, value_pre, gate_pre = (
        running.astype(jnp.bfloat16) for running in totals
    )
    heads_here = prior_state.shape[1]
    head_shape = (batch_rows, heads_here, HEAD_DIM)
    query_act = jax.nn.silu(query_pre.astype(jnp.float32)).reshape(head_shape)
    lower_bound = forget_floor.reshape(heads_here, HEAD_DIM)
    forget = lower_bound + (1.0 - lower_bound) * jax.nn.sigmoid(
        forget_pre.astype(jnp.float32).reshape(head_shape)
    )
    values_in = value_pre.astype(jnp.float32).reshape(head_shape)
    new_state = (
        forget[..., None] * prior_state + (1.0 - forget)[..., None] * values_in[:, :, None, :]
    )
    readout = jnp.einsum("bhk,bhkv->bhv", query_act, new_state, precision=lax.Precision.HIGHEST)
    gate_act = jax.nn.sigmoid(gate_pre.astype(jnp.float32).reshape(head_shape))
    gated_out = (
        readout * inverse_norm(readout) * group_gain.reshape(heads_here, HEAD_DIM) * gate_act
    ).astype(jnp.bfloat16)
    gated_flat = gated_out.reshape(batch_rows, heads_here * HEAD_DIM)
    mixed_part = jnp.dot(
        gated_flat,
        lax.all_gather(w_mix_out, "tp", axis=1, tiled=True),
        preferred_element_type=jnp.float32,
    )
    mixed_sum = summed_on_arrival(mixed_part, "kv", 1)
    mix_total = taken_together(jnp.sum(mixed_sum * mixed_sum, axis=1), "kv")
    mix_scale = lax.rsqrt(mix_total / full_width + epsilon)[:, None]
    post_gain = lax.dynamic_slice_in_dim(gain_mix_post, offset, own_cols, 0)
    after_mix = (residual.astype(jnp.float32) + mixed_sum * mix_scale * post_gain).astype(
        jnp.bfloat16
    )
    after_wide = after_mix.astype(jnp.float32)
    stream_total = lax.psum(jnp.sum(after_wide * after_wide, axis=1), "kv")
    stream_scale = lax.rsqrt(stream_total / full_width + epsilon)[:, None]
    pre_gain = lax.dynamic_slice_in_dim(gain_mlp_pre, offset, own_cols, 0)
    hidden_own = (after_wide * stream_scale * pre_gain).astype(jnp.bfloat16)
    hidden_in = lax.all_gather(hidden_own, "kv", axis=1, tiled=True)
    left_part = hidden_in
    up_sum = jnp.dot(
        left_part,
        lax.all_gather(w_up, "tp", axis=0, tiled=True),
        preferred_element_type=jnp.float32,
    )
    squared = jnp.square(jax.nn.relu(up_sum)).astype(jnp.bfloat16)
    channel_part = jnp.dot(
        squared,
        lax.all_gather(w_down, "tp", axis=1, tiled=True),
        preferred_element_type=jnp.float32,
    )
    out_gain = lax.dynamic_slice_in_dim(gain_mlp_post, offset, own_cols, 0)
    own_part = summed_on_arrival(channel_part, "kv", 1)
    layer_out = (after_mix.astype(jnp.float32) + own_part * out_gain).astype(jnp.bfloat16)
    return (layer_out, new_state)


def solution(mesh):
    return jax.shard_map(
        shards,
        mesh=mesh,
        in_specs=(
            P("tp", "kv"),
            P("tp", "kv", None, None),
            P("tp", "kv"),
            P("tp", "kv"),
            P("tp", "kv"),
            P("tp", "kv"),
            P("kv"),
            P("kv"),
            P("kv", "tp"),
            P(),
            P(),
            P(),
            P(),
            P("tp", "kv"),
            P("kv", "tp"),
        ),
        out_specs=(P("tp", "kv"), P("tp", "kv", None, None)),
        check_vma=False,
    )
```

profile of v0, /device:TPU:1, one launch (start us, length us, event | category | flops | bytes accessed | tf_op | source)
XLA Modules:
  0.0 254.0 jit_solution(2061126913411901489)
XLA Ops:
  7.2 0.0 copy-start.5
  7.2 0.0 copy-start.3
  7.2 0.0 copy-start.1
  7.2 0.0 all-gather.4.cloned.1.call-start
  7.2 1.5 pad_maximum_fusion
  8.7 0.0 all-gather.4.cloned.1.call-update
  8.8 0.0 all-gather.6.cloned.1.call-start
  8.8 0.7 all-gather.6.cloned.1.call-update
  9.5 0.0 all-gather.8.cloned.1.call-start
  9.6 0.7 all-gather.8.cloned.1.call-update
  10.2 19.4 %all_gather.18 = bf16[16,2048]{1,0:T(8,128)(2,1)S(1)} all-gather(bf16[16,128]{1,0:T(8,128)(2,1)} %param.15), channel_id=1, replica_groups=mesh['kv'=16,'tp'=32] {'kv'}, dimensions={1}, use_global_device_ids=true | all-gather | bytes 69632 | tf_op jit(solution)/shard_map/all_gather | solution.py:65
  29.7 0.1 fusion.26
  29.8 0.7 broadcast_subtract_fusion.1
  30.5 44.0 %all_gather.20 = bf16[128,2048]{0,1:T(8,128)(2,1)S(1)} all-gather(bf16[128,64]{0,1:T(8,128)(2,1)} %param.23), channel_id=1, replica_groups=mesh['kv'=16,'tp'=32] {'tp'}, dimensions={1}, use_global_device_ids=true | all-gather | bytes 540672 | tf_op jit(solution)/shard_map/all_gather | solution.py:99
  74.5 13.5 %all-gather.4.cloned.1.call-done = bf16[2048,512]{1,0:T(8,128)(2,1)} async-done(((bf16[64,512]{1,0:T(8,128)(2,1)}), bf16[2048,512]{1,0:T(8,128)(2,1)}) %all-gather.4.cloned.1.call-update) | async-done | bytes 2097168 | tf_op jit(solution)/shard_map/all_gather | solution.py:15
  87.9 1.3 fusion.9
  89.2 1.3 divide_multiply_fusion
  90.5 0.0 copy-done.5
  90.6 0.0 copy-done.3
  90.6 0.0 copy-start.4
  90.6 1.3 broadcast_subtract_fusion
  91.9 0.0 copy-done.1
  91.9 0.0 copy-start.2
  91.9 0.6 multiply_add_fusion
  92.5 0.0 copy-start
  92.5 1.0 fusion.19
  93.5 0.1 multiply_reduce_fusion.1
  93.6 0.0 copy-done.4
  93.6 1.5 convolution_bitcast_fusion
  95.1 13.2 %all_to_all.16 = f32[16,16,128]{2,1,0:T(8,128)S(1)} all-to-all(f32[16,16,128]{2,1,0:T(8,128)S(1)} %convolution_bitcast_fusion), channel_id=1, replica_groups=mesh['kv'=16,'tp'=32] {'kv'}, dimensions={0} | all-to-all | bytes 262144 | tf_op jit(solution)/shard_map/all_to_all | solution.py:26
  108.4 0.1 multiply_reduce_fusion
  108.5 0.6 broadcast_in_dim.2
  109.1 3.4 %all-to-all-start.1 = ((f32[16,1,16]{2,1,0:T(1,128)}), f32[16,1,16]{2,1,0:T(1,128)S(1)}, u32[]{:S(2)}, u32[]{:S(2)}) async-start(f32[16,1,16]{2,1,0:T(1,128)} %broadcast_in_dim.2), calls=%async_computation.1 | async-start | bytes 16384 | tf_op jit(solution)/shard_map/all_to_all | solution.py:32
  112.6 0.8 dynamic_slice.9
  113.3 0.8 dynamic_slice.10
  114.1 4.7 %all-to-all-done.1 = f32[16,1,16]{2,1,0:T(1,128)S(1)} async-done(((f32[16,1,16]{2,1,0:T(1,128)}), f32[16,1,16]{2,1,0:T(1,128)S(1)}, u32[]{:S(2)}, u32[]{:S(2)}) %all-to-all-start.1) | async-done | bytes 1056 | tf_op jit(solution)/shard_map/all_to_all | solution.py:32
  118.8 0.2 fusion.30
  119.0 30.4 %psum.7 = f32[16]{0:T(128)S(1)} all-reduce(f32[16]{0:T(128)S(1)} %get-tuple-element.2), channel_id=1, replica_groups=mesh['kv'=16,'tp'=32] {'kv'}, use_global_device_ids=true, to_apply=%region_6.7 | all-reduce | flops 16 | bytes 128 | tf_op jit(solution)/shard_map/psum | solution.py:110
  149.4 0.1 fusion.32
  149.5 16.5 %all_gather.21 = bf16[16,2048]{1,0:T(8,128)(2,1)S(1)} all-gather(bf16[16,128]{1,0:T(8,128)(2,1)S(1)} %fusion.32), channel_id=1, replica_groups=mesh['kv'=16,'tp'=32] {'kv'}, dimensions={1}, use_global_device_ids=true | all-gather | bytes 69632 | tf_op jit(solution)/shard_map/all_gather | solution.py:114
  166.0 0.0 all-gather.6.cloned.1.call-done
  166.0 63.7 %all-gather.8.cloned.1.call-done = bf16[512,2048]{0,1:T(8,128)(2,1)} async-done(((bf16[512,64]{0,1:T(8,128)(2,1)}), bf16[512,2048]{0,1:T(8,128)(2,1)}) %all-gather.8.cloned.1.call-update) | async-done | bytes 2097168 | tf_op jit(solution)/shard_map/all_gather | solution.py:124
  229.7 3.2 %convolution_bitcast_fusion.1 = f32[2,16,8,128]{3,2,1,0:T(8,128)S(1)} fusion(bf16[512,2048]{0,1:T(8,128)(2,1)} %all-gather.8.cloned.1.call-done, bf16[16,2048]{1,0:T(8,128)(2,1)S(1)} %all_gather.21, bf16[2048,512]{1,0:T(8,128)(2,1)} %all-gather.6.cloned.1.call-done), kind=kOutput, calls=%fused_computation.1 | convolution fusion | flops 67133440 | bytes 4390912 | tf_op jit(solution)/shard_map/dot_general | solution.py:122
  232.9 0.7 copy.25
  233.5 6.5 %all-to-all-start.2 = ((f32[16,16,128]{2,1,0:T(8,128)}), f32[16,16,128]{2,1,0:T(8,128)S(1)}, u32[]{:S(2)}, u32[]{:S(2)}) async-start(f32[16,16,128]{2,1,0:T(8,128)} %bitcast.30), calls=%async_computation.2 | async-start | bytes 262144 | tf_op jit(solution)/shard_map/all_to_all | solution.py:26
  240.1 0.8 dynamic_slice.11
  240.8 6.1 %all-to-all-done.2 = f32[16,16,128]{2,1,0:T(8,128)S(1)} async-done(((f32[16,16,128]{2,1,0:T(8,128)}), f32[16,16,128]{2,1,0:T(8,128)S(1)}, u32[]{:S(2)}, u32[]{:S(2)}) %all-to-all-start.2) | async-done | bytes 131104 | tf_op jit(solution)/shard_map/all_to_all | solution.py:26
  246.9 0.6 fusion.33
  (9 shorter events, 0.1 us)
Async XLA Ops:
  7.2 83.4 %copy-start.5 = (f32[128]{0:T(128)S(1)}, f32[128]{0:T(128)}, u32[]{:S(2)}) copy-start(f32[128]{0:T(128)} %param.21) | copy-start | bytes 1540
  7.2 83.4 %copy-start.3 = (f32[2048]{0:T(1024)S(1)}, f32[2048]{0:T(1024)}, u32[]{:S(2)}) copy-start(f32[2048]{0:T(1024)} %param.24) | copy-start | bytes 24580
  7.2 84.7 %copy-start.1 = (f32[16,1,128,128]{3,2,1,0:T(8,128)S(1)}, f32[16,1,128,128]{3,2,1,0:T(8,128)}, u32[]{:S(2)}) copy-start(f32[16,1,128,128]{3,2,1,0:T(8,128)} %param.16) | copy-start | bytes 3145732
  7.2 80.7 %all-gather.4.cloned.1.call-start = ((), (), s32[]{:S(2)}) async-start(), calls=%async_computation.3 | async-start | bytes 2162688 | tf_op jit(solution)/shard_map/all_gather | solution.py:15
  8.8 157.2 %all-gather.6.cloned.1.call-start = ((), (), s32[]{:S(2)}) async-start(), calls=%async_computation.4 | async-start | bytes 2162688 | tf_op jit(solution)/shard_map/all_gather | solution.py:118
  9.5 220.2 %all-gather.8.cloned.1.call-start = ((), (), s32[]{:S(2)}) async-start(), calls=%async_computation.5 | async-start | bytes 2162688 | tf_op jit(solution)/shard_map/all_gather | solution.py:124
  90.6 3.1 %copy-start.4 = (f32[128]{0:T(128)S(1)}, f32[128]{0:T(128)}, u32[]{:S(2)}) copy-start(f32[128]{0:T(128)} %param.22) | copy-start | bytes 1540
  91.9 26.9 %copy-start.2 = (bf16[16,128]{1,0:T(8,128)(2,1)S(1)}, bf16[16,128]{1,0:T(8,128)(2,1)}, u32[]{:S(2)}) copy-start(bf16[16,128]{1,0:T(8,128)(2,1)} %param.15) | copy-start | bytes 12292
  92.5 140.3 %copy-start = (f32[16,1,128,128]{3,2,1,0:T(8,128)}, f32[16,1,128,128]{3,2,1,0:T(8,128)S(1)}, u32[]{:S(2)}) copy-start(f32[16,1,128,128]{3,2,1,0:T(8,128)S(1)} %multiply_add_fusion) | copy-start | bytes 3145732
  109.1 9.7 %all-to-all-start.1 = ((f32[16,1,16]{2,1,0:T(1,128)}), f32[16,1,16]{2,1,0:T(1,128)S(1)}, u32[]{:S(2)}, u32[]{:S(2)}) async-start(f32[16,1,16]{2,1,0:T(1,128)} %broadcast_in_dim.2), calls=%async_computation.1 | async-start | bytes 16384 | tf_op jit(solution)/shard_map/all_to_all | solution.py:32
  233.5 13.4 %all-to-all-start.2 = ((f32[16,16,128]{2,1,0:T(8,128)}), f32[16,16,128]{2,1,0:T(8,128)S(1)}, u32[]{:S(2)}, u32[]{:S(2)}) async-start(f32[16,16,128]{2,1,0:T(8,128)} %bitcast.30), calls=%async_computation.2 | async-start | bytes 262144 | tf_op jit(solution)/shard_map/all_to_all | solution.py:26
Sparse Core Ops, SparseCore 0:
  10.7 77.1 all-gather.3
  90.1 68.8 all-gather.5
  161.1 68.5 all-gather.7
where the time goes:
time: 255 us; the launch traced here: 254 us
  blocking collectives  124 us (49%)
  waiting for transfers between devices  89.3 us (35%)
  between operations  13.9 us (5%)
  starting transfers between devices  10.1 us (4%)
  matrix products  9.56 us (4%)
  other arithmetic  4.07 us (2%)
  local copies, waits for them, and re-layouts  3.6 us (1%)
    all_gather x1, waiting for transfers between devices, shards(): lax.all_gather(w_down, 'tp', axis=1, tiled=True)  63.7 us
    all_gather x1, blocking collectives, shards(): lax.all_gather(w_mix_out, 'tp', axis=1, tiled=True)  44 us
    psum x1, blocking collectives, shards(): stream_total = lax.psum(jnp.sum(after_wide * after_wide, axis=1), 'kv')  30.4 us
    all_gather x1, blocking collectives, shards(): whole_rows = lax.all_gather(residual, 'kv', axis=1, tiled=True)  19.4 us
    all_gather x1, blocking collectives, shards(): hidden_in = lax.all_gather(hidden_own, 'kv', axis=1, tiled=True)  16.5 us
    all_gather x1, waiting for transfers between devices, side_by_side(): filled = lax.all_gather(both, axis, axis=dim, tiled=True)  13.5 us
    all_to_all x1, blocking collectives, summed_on_arrival(): lax.all_to_all(split_up(value, dim, devices), axis, 0, 0, tiled=True)  13.2 us
    all_to_all x1, starting transfers between devices, summed_on_arrival(): lax.all_to_all(split_up(value, dim, devices), axis, 0, 0, tiled=True)  6.53 us
  transfers between devices with their start and end apart: 5, of which 4 were waited for; matrix products, arithmetic and copies ran while one was open for 4% of the time, Pallas kernels for 0%

commit v1 on v0

v1 whole, which is shorter than its diff:
```python
import jax
import jax.numpy as jnp
from jax import lax
from jax.sharding import Mesh
from jax.sharding import PartitionSpec as P

HEAD_DIM = 128
KV = ("y", "x")
TP = ("z", "c")

epsilon = 1e-06


def inverse_norm(values):
    return lax.rsqrt(jnp.mean(values * values, axis=-1, keepdims=True) + epsilon)


def exchange(blocks, axes):
    return lax.all_to_all(blocks, axes, 0, 0, tiled=True)


def from_everyone(value, axes):
    devices = lax.axis_size(axes)
    return exchange(jnp.broadcast_to(value[None], (devices, *value.shape)), axes)


def shards(
    residual,
    prior_state,
    w_query,
    w_forget,
    w_value,
    w_outgate,
    forget_floor,
    group_gain,
    w_mix_out,
    gain_mix_pre,
    gain_mix_post,
    gain_mlp_pre,
    gain_mlp_post,
    w_up,
    w_down,
):
    batch_rows, own_cols = residual.shape
    groups = lax.axis_size(KV)
    full_width = groups * own_cols
    place = lax.axis_index(KV)
    head_cols = w_query.shape[1]
    hidden = w_up.shape[1]

    own_weights = jnp.concatenate(
        (w_query, w_forget, w_value, w_outgate, w_mix_out.T, w_up, w_down.T), axis=1
    )
    weights = lax.all_gather(own_weights, TP, axis=0, tiled=True)
    at = 4 * head_cols
    w_in = weights[:, :at]
    w_mix = weights[:, at : at + w_mix_out.shape[0]]
    at += w_mix_out.shape[0]
    w_up_all = weights[:, at : at + hidden]
    w_down_all = weights[:, at + hidden :]

    stream = from_everyone(residual, KV).astype(jnp.float32)
    scale = lax.rsqrt(
        jnp.sum(stream * stream, axis=(0, 2), keepdims=True) / full_width + epsilon
    )
    normed = (stream * scale * gain_mix_pre.reshape(groups, 1, own_cols)).astype(jnp.bfloat16)
    normed = normed.transpose(1, 0, 2).reshape(batch_rows, full_width)
    pre = jnp.dot(normed, w_in, preferred_element_type=jnp.float32).astype(jnp.bfloat16)
    query_pre, forget_pre, value_pre, gate_pre = (
        p.astype(jnp.float32) for p in jnp.split(pre, 4, axis=1)
    )
    query = jax.nn.silu(query_pre)
    forget = forget_floor + (1.0 - forget_floor) * jax.nn.sigmoid(forget_pre)
    new_state = (
        forget[:, :, None] * prior_state[:, 0]
        + (1.0 - forget)[:, :, None] * value_pre[:, None, :]
    )
    readout = jnp.einsum("bk,bkv->bv", query, new_state, precision=lax.Precision.HIGHEST)
    gated = (
        readout * inverse_norm(readout) * group_gain * jax.nn.sigmoid(gate_pre)
    ).astype(jnp.bfloat16)
    mixed_part = lax.dot_general(
        gated, w_mix, (((1,), (1,)), ((), ())), preferred_element_type=jnp.float32
    )
    mixed = exchange(
        mixed_part.astype(jnp.bfloat16).reshape(batch_rows, groups, own_cols), KV
    )
    mixed = jnp.sum(mixed.astype(jnp.float32), axis=0)
    mix_scale = lax.rsqrt(jnp.sum(mixed * mixed) / full_width + epsilon)
    own_row = lax.dynamic_index_in_dim(stream, place, 1, keepdims=False)
    after_row = (
        own_row + mixed * mix_scale * gain_mix_post.reshape(groups, own_cols)
    ).astype(jnp.bfloat16)
    after = from_everyone(after_row, KV).astype(jnp.float32)
    after_scale = lax.rsqrt(
        jnp.sum(after * after, axis=(1, 2), keepdims=True) / full_width + epsilon
    )
    hidden_in = (after * after_scale * gain_mlp_pre.reshape(groups, own_cols)).astype(
        jnp.bfloat16
    )
    up_sum = jnp.dot(
        hidden_in.reshape(batch_rows, full_width), w_up_all, preferred_element_type=jnp.float32
    )
    squared = jnp.square(jax.nn.relu(up_sum)).astype(jnp.bfloat16)
    channel_part = lax.dot_general(
        squared, w_down_all, (((1,), (1,)), ((), ())), preferred_element_type=jnp.float32
    )
    channel = exchange(
        channel_part.astype(jnp.bfloat16)
        .reshape(batch_rows, groups, own_cols)
        .transpose(1, 0, 2),
        KV,
    )
    channel = jnp.sum(channel.astype(jnp.float32), axis=0)
    out_gain = lax.dynamic_index_in_dim(
        gain_mlp_post.reshape(groups, own_cols), place, 0, keepdims=True
    )
    after_own = lax.dynamic_index_in_dim(after, place, 1, keepdims=False)
    layer_out = (after_own + channel * out_gain).astype(jnp.bfloat16)
    return layer_out, new_state[:, None]


def solution(mesh):
    grid = Mesh(mesh.devices.reshape(4, 4, 16, 2), (*KV, *TP))
    return jax.shard_map(
        shards,
        mesh=grid,
        in_specs=(
            P(TP, KV),
            P(TP, KV, None, None),
            P(TP, KV),
            P(TP, KV),
            P(TP, KV),
            P(TP, KV),
            P(KV),
            P(KV),
            P(KV, TP),
            P(),
            P(),
            P(),
            P(),
            P(TP, KV),
            P(KV, TP),
        ),
        out_specs=(P(TP, KV), P(TP, KV, None, None)),
        check_vma=False,
    )
```

time: 255 us -> 154 us (0.60)
  the two profiles are of different devices: /device:TPU:1 before, /device:TPU:32 now
where the time goes in v1:
time: 154 us; the launch traced here: 153 us
  waiting for transfers between devices  92.2 us (60%)
  starting transfers between devices  20.9 us (14%)
  between operations  14.8 us (10%)
  local copies, waits for them, and re-layouts  9.3 us (6%)
  matrix products  9.19 us (6%)
  other arithmetic  6.68 us (4%)
    all_gather x1, waiting for transfers between devices, shards(): weights = lax.all_gather(own_weights, TP, axis=0, tiled=True)  65.2 us
    all_to_all x4, waiting for transfers between devices, exchange(): return lax.all_to_all(blocks, axes, 0, 0, tiled=True)  27 us
    all_to_all x4, starting transfers between devices, exchange(): return lax.all_to_all(blocks, axes, 0, 0, tiled=True)  20.8 us
    unnamed x13, local copies, waits for them, and re-layouts  5.83 us
    dot_general x1, matrix products, shards(): lax.dot_general(squared, w_down_all, (((1,), (1,)), ((), ())), preferred_...  3.21 us
  transfers between devices with their start and end apart: 5, of which 5 were waited for; matrix products, arithmetic and copies ran while one was open for 3% of the time, Pallas kernels for 0%

profile of v1, /device:TPU:32, one launch (start us, length us, event | category | flops | bytes accessed | tf_op | source)
XLA Modules:
  0.0 153.1 jit_solution(12552396937788839422)
XLA Ops:
  7.2 0.0 copy-start
  7.2 0.0 copy-start.2
  7.2 0.0 all-gather.2.cloned.1.call-start
  7.2 0.7 constant_dynamic-update-slice_fusion.5
  8.0 0.7 constant_dynamic-update-slice_fusion.4
  8.7 0.7 constant_dynamic-update-slice_fusion.3
  9.4 0.7 constant_dynamic-update-slice_fusion.2
  10.1 0.7 constant_dynamic-update-slice_fusion.1
  10.9 0.8 constant_dynamic-update-slice_fusion
  11.7 0.8 bitcast_dynamic-update-slice_fusion
  12.6 0.0 copy-start.1
  12.6 0.7 copy-done.1
  13.2 0.0 all-gather.2.cloned.1.call-update
  13.3 1.3 broadcast_in_dim.4
  14.6 7.0 %all-to-all-start = ((bf16[16,16,128]{2,1,0:T(8,128)(2,1)}), bf16[16,16,128]{2,1,0:T(8,128)(2,1)S(1)}, u32[]{:S(2)}, u32[]{:S(2)}) async-start(bf16[16,16,128]{2,1,0:T(8,128)(2,1)} %broadcast_in_dim.4), calls=%async_computation | async-start | bytes 131072 | tf_op jit(solution)/shard_map/all_to_all | solution.py:19
  21.6 0.7 broadcast_subtract_fusion.1
  22.3 0.0 copy-done
  22.3 7.0 %all-to-all-done = bf16[16,16,128]{2,1,0:T(8,128)(2,1)S(1)} async-done(((bf16[16,16,128]{2,1,0:T(8,128)(2,1)}), bf16[16,16,128]{2,1,0:T(8,128)(2,1)S(1)}, u32[]{:S(2)}, u32[]{:S(2)}) %all-to-all-start) | async-done | bytes 65568 | tf_op jit(solution)/shard_map/all_to_all | solution.py:19
  29.3 0.1 multiply_reduce_fusion.1
  29.4 65.2 %all-gather.2.cloned.1.call-done = bf16[2048,1664]{1,0:T(8,128)(2,1)} async-done(((bf16[64,1664]{1,0:T(8,128)(2,1)}), bf16[2048,1664]{1,0:T(8,128)(2,1)}) %all-gather.2.cloned.1.call-update) | async-done | bytes 6815760 | tf_op jit(solution)/shard_map/all_gather | solution.py:54
  94.7 2.0 %fusion.20 = bf16[16,512]{1,0:T(8,128)(2,1)S(1)} fusion(bf16[2048,1664]{1,0:T(8,128)(2,1)} %all-gather.2.cloned.1.call-done, f32[16,128]{1,0:T(8,128)} %bitcast.60, f32[16]{0:T(128)S(1)} %add_rsqrt_fusion.2, bf16[16,16,128]{2,1,0:T(8,128)(2,1)S(1)} %all-to-all-done), kind=kOutput, calls=%fused_computation.12 | convolution fusion | flops 33693696 | bytes 2187328 | tf_op jit(solution)/shard_map/dot_general | solution.py:68
  96.7 0.7 multiply_add_fusion.1
  97.4 2.6 %fusion.24 = f32[16,1,128]{2,1,0:T(1,128)S(1)} fusion(f32[16,128,1]{1,2,0:T(1,128)S(1)} %bitcast.56, f32[16,1,128,128]{3,2,1,0:T(8,128)} %param.16, f32[16,128]{1,0:T(8,128)S(1)} %slice_convert_fusion, f32[16,128]{1,0:T(8,128)S(1)} %get-tuple-element.3, f32[16,128]{1,0:T(8,128)S(1)} %get-tuple-element.2), kind=kOutput, calls=%fused_computation.15 | convolution fusion | flops 3932160 | bytes 1089536 | tf_op jit(solution)/shard_map/bk,bkv->bv/dot_general | solution.py:78
  100.0 0.1 multiply_reduce_fusion.3
  100.1 1.3 fusion.8
  101.5 0.7 copy.24
  102.1 6.8 %all-to-all-start.1 = ((bf16[16,16,128]{2,1,0:T(8,128)(2,1)}), bf16[16,16,128]{2,1,0:T(8,128)(2,1)S(1)}, u32[]{:S(2)}, u32[]{:S(2)}) async-start(bf16[16,16,128]{2,1,0:T(8,128)(2,1)} %bitcast.22), calls=%async_computation.1 | async-start | bytes 131072 | tf_op jit(solution)/shard_map/all_to_all | solution.py:19
  109.0 7.6 %all-to-all-done.1 = bf16[16,16,128]{2,1,0:T(8,128)(2,1)S(1)} async-done(((bf16[16,16,128]{2,1,0:T(8,128)(2,1)}), bf16[16,16,128]{2,1,0:T(8,128)(2,1)S(1)}, u32[]{:S(2)}, u32[]{:S(2)}) %all-to-all-start.1) | async-done | bytes 65568 | tf_op jit(solution)/shard_map/all_to_all | solution.py:19
  116.6 0.6 multiply_reduce_fusion.2
  117.9 0.7 fusion.43
  118.6 0.6 broadcast_in_dim.5
  119.3 3.5 %all-to-all-start.2 = ((bf16[16,16,128]{2,1,0:T(8,128)(2,1)}), bf16[16,16,128]{2,1,0:T(8,128)(2,1)S(1)}, u32[]{:S(2)}, u32[]{:S(2)}) async-start(bf16[16,16,128]{2,1,0:T(8,128)(2,1)} %broadcast_in_dim.5), calls=%async_computation.2 | async-start | bytes 131072 | tf_op jit(solution)/shard_map/all_to_all | solution.py:19
  122.8 2.8 %multiply_add_fusion = f32[16,1,128,128]{3,2,1,0:T(8,128)} fusion(f32[16,1,128,128]{3,2,1,0:T(8,128)} %param.16, f32[16,128]{1,0:T(8,128)S(1)} %slice_convert_fusion, f32[16,128]{1,0:T(8,128)S(1)} %get-tuple-element.3, f32[16,128]{1,0:T(8,128)S(1)} %get-tuple-element.2), kind=kLoop, calls=%fused_computation.16 | loop fusion | flops 786432 | bytes 2121728 | tf_op jit(solution)/shard_map/add | solution.py:75
  125.6 4.8 %all-to-all-done.2 = bf16[16,16,128]{2,1,0:T(8,128)(2,1)S(1)} async-done(((bf16[16,16,128]{2,1,0:T(8,128)(2,1)}), bf16[16,16,128]{2,1,0:T(8,128)(2,1)S(1)}, u32[]{:S(2)}, u32[]{:S(2)}) %all-to-all-start.2) | async-done | bytes 65568 | tf_op jit(solution)/shard_map/all_to_all | solution.py:19
  130.4 0.2 multiply_reduce_fusion
  130.6 0.0 copy-done.2
  130.6 0.1 multiply_convert_fusion
  130.7 3.2 %fusion.5 = bf16[2,16,8,128]{3,2,1,0:T(8,128)(2,1)S(1)} fusion(bf16[2048,1664]{1,0:T(8,128)(2,1)} %all-gather.2.cloned.1.call-done, bf16[2,8,16,128]{3,2,1,0:T(8,128)(2,1)S(1)} %bitcast.53), kind=kOutput, calls=%fused_computation.7 | convolution fusion | flops 67166208 | bytes 4325376 | tf_op jit(solution)/shard_map/dot_general | solution.py:105
  133.9 0.6 copy.36
  134.6 3.5 %all-to-all-start.3 = ((bf16[16,16,128]{2,1,0:T(8,128)(2,1)}), bf16[16,16,128]{2,1,0:T(8,128)(2,1)S(1)}, u32[]{:S(2)}, u32[]{:S(2)}) async-start(bf16[16,16,128]{2,1,0:T(8,128)(2,1)} %bitcast.51), calls=%async_computation.3 | async-start | bytes 131072 | tf_op jit(solution)/shard_map/all_to_all | solution.py:19
  138.1 7.6 %all-to-all-done.3 = bf16[16,16,128]{2,1,0:T(8,128)(2,1)S(1)} async-done(((bf16[16,16,128]{2,1,0:T(8,128)(2,1)}), bf16[16,16,128]{2,1,0:T(8,128)(2,1)S(1)}, u32[]{:S(2)}, u32[]{:S(2)}) %all-to-all-start.3) | async-done | bytes 65568 | tf_op jit(solution)/shard_map/all_to_all | solution.py:19
  145.7 0.6 add_convert_fusion
  (11 shorter events, 0.1 us)
Async XLA Ops:
  7.2 15.1 %copy-start = (f32[2048]{0:T(1024)S(1)}, f32[2048]{0:T(1024)}, u32[]{:S(2)}) copy-start(f32[2048]{0:T(1024)} %param.27) | copy-start | bytes 24580
  7.2 123.4 %copy-start.2 = (f32[2048]{0:T(1024)S(1)}, f32[2048]{0:T(1024)}, u32[]{:S(2)}) copy-start(f32[2048]{0:T(1024)} %param.26) | copy-start | bytes 24580
  7.2 87.5 %all-gather.2.cloned.1.call-start = ((), (), s32[]{:S(2)}) async-start(), calls=%async_computation.4 | async-start | bytes 7028736 | tf_op jit(solution)/shard_map/all_gather | solution.py:54
  12.6 0.7 copy-start.1
  14.6 14.7 %all-to-all-start = ((bf16[16,16,128]{2,1,0:T(8,128)(2,1)}), bf16[16,16,128]{2,1,0:T(8,128)(2,1)S(1)}, u32[]{:S(2)}, u32[]{:S(2)}) async-start(bf16[16,16,128]{2,1,0:T(8,128)(2,1)} %broadcast_in_dim.4), calls=%async_computation | async-start | bytes 131072 | tf_op jit(solution)/shard_map/all_to_all | solution.py:19
  102.1 14.5 %all-to-all-start.1 = ((bf16[16,16,128]{2,1,0:T(8,128)(2,1)}), bf16[16,16,128]{2,1,0:T(8,128)(2,1)S(1)}, u32[]{:S(2)}, u32[]{:S(2)}) async-start(bf16[16,16,128]{2,1,0:T(8,128)(2,1)} %bitcast.22), calls=%async_computation.1 | async-start | bytes 131072 | tf_op jit(solution)/shard_map/all_to_all | solution.py:19
  119.3 11.1 %all-to-all-start.2 = ((bf16[16,16,128]{2,1,0:T(8,128)(2,1)}), bf16[16,16,128]{2,1,0:T(8,128)(2,1)S(1)}, u32[]{:S(2)}, u32[]{:S(2)}) async-start(bf16[16,16,128]{2,1,0:T(8,128)(2,1)} %broadcast_in_dim.5), calls=%async_computation.2 | async-start | bytes 131072 | tf_op jit(solution)/shard_map/all_to_all | solution.py:19
  134.6 11.1 %all-to-all-start.3 = ((bf16[16,16,128]{2,1,0:T(8,128)(2,1)}), bf16[16,16,128]{2,1,0:T(8,128)(2,1)S(1)}, u32[]{:S(2)}, u32[]{:S(2)}) async-start(bf16[16,16,128]{2,1,0:T(8,128)(2,1)} %bitcast.51), calls=%async_computation.3 | async-start | bytes 131072 | tf_op jit(solution)/shard_map/all_to_all | solution.py:19
Sparse Core Ops, SparseCore 0:
  13.4 81.2 all-gather.1
